TPU v7x, 512 devices: a whole 4x4x16 slice. The times are simulated.
512 devices in a mesh: sp: 128 (over z, x, core), tp: 4 (over y).
Axes of the slice: x: 4, y: 4, z: 16, core: 2. Of those that a mesh axis runs over, the one named last changes fastest.
Arguments:
- conv_gate: bfloat16 [32768, 512], P('sp', 'tp'), may hold values from -6 to 6
- conv_mix: bfloat16 [32768, 512], P('sp', 'tp'), may hold values from -6 to 6
- conv_input: bfloat16 [32768, 512], P('sp', 'tp'), may hold values from -6 to 6
- conv_taps: bfloat16 [3, 512], P(None, 'tp'), may hold values from -3.5 to 3.5
- query_rows: bfloat16 [32768, 512], P('sp', 'tp'), may hold values from -50 to 50, as said below
- key_rows: bfloat16 [32768, 512], P('sp', 'tp'), may hold values from -10 to 10, as said below
- value_rows: bfloat16 [32768, 512], P('sp', 'tp'), may hold values from -6 to 6
- lambdas: float32 [4], P('tp'), may hold values from 0.3 to 0.8
- head_gain: float32 [128], replicated, may hold values from 0.1 to 1.9
- w_out_conv: bfloat16 [512, 2048], P('tp'), may hold values from -0.1875 to 0.1875
- w_out_heads: bfloat16 [512, 2048], P('tp'), may hold values from -0.1875 to 0.1875
Outputs:
- mixed: bfloat16 [32768, 2048], P(('sp', 'tp'))
Inputs may be any that keep to these rules, and one draw needn't show every extreme that they name: `query_rows`: queries of order one; some rows may be far larger. `key_rows`: keys of order one.
All inputs are finite; a program needn't handle non-finite values.
Results may differ from a plain program's by a relative error of at most 0.013.
Values may be sent and summed in bfloat16 or wider, within the bound.
No kernel may reach another device: no remote copies, remote signals or barrier semaphores. Data moves between devices by JAX's collectives and lax.ppermute only.
A program may use at most 128 MiB of HBM per device.

v0:
```python
import math

import jax
import jax.numpy as jnp
from jax import lax
from jax.experimental import pallas as pl
from jax.experimental.pallas import tpu as pltpu
from jax.sharding import PartitionSpec as P


f32, bf16 = jnp.float32, jnp.bfloat16
HEAD_QK = 64
HEAD_V = 128
MAPS = 2
PLANES = 16
CORES = 2
Q_STEP = 256
K_STEP = 512
SCALE = HEAD_QK**-0.5 * math.log2(math.e)
LOW = -1e30
MASKED = -2e30
STAT = 16
OUT_ROWS = HEAD_V + 8
NN = (((1,), (0,)), ((), ()))


def pack_kernel(q_ref, k_ref, v_ref, pair_ref, copies_ref):
    pair_ref[:, :HEAD_V] = k_ref[...]
    pair_ref[:, HEAD_V:] = v_ref[...]
    for i in range(copies_ref.shape[0]):
        copies_ref[i] = q_ref[...]


def pack(q, k, v, copies):
    rows, width = q.shape
    return pl.pallas_call(
        pack_kernel,
        out_shape=[
            jax.ShapeDtypeStruct((rows, 2 * width), bf16),
            jax.ShapeDtypeStruct((copies, rows, width), bf16),
        ],
        name="pack",
    )(q, k, v)


def flash_kernel(rows, at, lam, q_ref, kv_hbm, out_hbm, *refs):
    kv_ref, out_ref, kv_sems, out_sems, m_s, acc, qt, s_a, s_b, b_a, b_b = refs
    full = at[0]
    end = full + 1

    def come(i):
        part = pl.ds(i * K_STEP, K_STEP)
        return pltpu.make_async_copy(kv_hbm.at[part], kv_ref.at[part], kv_sems.at[i])

    def fetch(i, _):
        come(i).start()
        return 0

    lax.fori_loop(0, end, fetch, 0)
    shards = q_ref.shape[0] // rows
    blocks = q_ref.shape[0] // Q_STEP
    lines = shards // 2
    e, x, c = at[1], at[2], at[3]

    def prepare(i, _):
        blk = q_ref[pl.ds(i * rows, rows), :].astype(f32).T * SCALE
        high = blk.astype(bf16).astype(f32)
        rest = blk - high
        for m in range(MAPS):
            lo, hi = HEAD_QK * m, HEAD_QK * (m + 1)
            qt[m, :, pl.ds(i * rows, rows)] = jnp.zeros((4 * HEAD_QK, rows), bf16)
            qt[m, lo:hi, pl.ds(i * rows, rows)] = high[lo:hi].astype(bf16)
            qt[m, 128 + lo : 128 + hi, pl.ds(i * rows, rows)] = rest[lo:hi].astype(bf16)
        return 0

    lax.fori_loop(0, shards, prepare, 0)
    m_s[...] = jnp.full(m_s.shape, LOW, f32)
    acc[...] = jnp.zeros(acc.shape, f32)
    scores = ((s_a, b_a), (s_b, b_b))

    def cols(b):
        return slice(b * Q_STEP, (b + 1) * Q_STEP)

    def score(i, b, ahead):
        s_ref, b_ref = scores[b % 2]
        k = kv_ref[pl.ds(i * K_STEP, K_STEP), :HEAD_V]
        k = jnp.concatenate([k, k], axis=1)
        for m in range(MAPS):
            s = lax.dot_general(k, qt[m, :, cols(b)], NN, preferred_element_type=f32)
            if ahead is not None:
                parts = []
                for h in range(Q_STEP // rows):
                    g = b * (Q_STEP // rows) + h
                    first = ((g // lines) * shards + (g % lines) * CORES + c) * rows
                    parts.append(jnp.where(ahead <= first, s[:, h * rows : (h + 1) * rows], MASKED))
                s = jnp.concatenate(parts, axis=1)
            s_ref[m] = s
            b_ref[m] = jnp.max(s.reshape(K_STEP // 8, 8, Q_STEP), axis=0)

    def weigh(v, b):
        s_ref, b_ref = scores[b % 2]
        for m in range(MAPS):
            old = m_s[m, :, cols(b)]
            new = jnp.maximum(old, jnp.max(b_ref[m], axis=0, keepdims=True))
            weights = jnp.exp2(s_ref[m] - new[:1]).astype(bf16)
            shrink = jnp.exp2(old - new)
            m_s[m, :, cols(b)] = new
            o = lax.dot_general(v, weights, NN, preferred_element_type=f32)
            acc[m, :, cols(b)] = acc[m, :, cols(b)] * shrink[:1] + o

    def values(i):
        v = kv_ref[pl.ds(i * K_STEP, K_STEP), HEAD_V:].astype(f32).T.astype(bf16)
        return jnp.concatenate([v, jnp.ones((STAT, K_STEP), bf16)], axis=0)

    come(0).wait()
    score(0, 0, None)

    def body(i, _):
        come(i + 1).wait()
        v = values(i)
        for b in range(blocks):
            if b + 1 < blocks:
                score(i, b + 1, None)
            else:
                score(i + 1, 0, None)
            weigh(v, b)
        return 0

    lax.fori_loop(0, full, body, 0)

    def edge(i, _):
        base = (e * shards + x * CORES) * rows
        ahead = (
            lax.broadcasted_iota(jnp.int32, (K_STEP, rows), 0)
            - lax.broadcasted_iota(jnp.int32, (K_STEP, rows), 1)
            + base
        )
        v = values(i)
        score(i, 0, ahead)
        for b in range(blocks):
            if b + 1 < blocks:
                score(i, b + 1, ahead)
            weigh(v, b)
        return 0

    lax.fori_loop(full, end, edge, 0)

    def leave(s):
        return pltpu.make_async_copy(out_ref.at[s], out_hbm.at[s], out_sems.at[s])

    def finish(s, _):
        at_cols = pl.ds(s * rows, rows)
        sides = []
        for m in range(MAPS):
            a = acc[m, :, at_cols]
            den = jnp.maximum(a[HEAD_V : HEAD_V + 8], 1e-30)
            factor = lam[0] / den[:1] if m else 1.0 / den[:1]
            rest = m_s[m, :, at_cols] + jnp.log2(den)
            parts = []
            for _ in range(3):
                hi = rest.astype(bf16).astype(f32)
                parts.append(hi)
                rest = rest - hi
            r = lax.broadcasted_iota(jnp.int32, rest.shape, 0)
            stat = jnp.where(r == 0, parts[0], jnp.where(r == 1, parts[1], parts[2]))
            sides.append(jnp.concatenate([a[:HEAD_V] * factor, stat], axis=0))
        for t in range(rows // 128):
            first = sides[0][:, t * 128 : (t + 1) * 128]
            second = pltpu.roll(sides[1][:, t * 128 : (t + 1) * 128], 64, 1)
            lower = lax.broadcasted_iota(jnp.int32, first.shape, 1) < 64
            out_ref[s, 2 * t] = jnp.where(lower, first, second).astype(bf16)
            out_ref[s, 2 * t + 1] = jnp.where(lower, second, first).astype(bf16)
        leave(s).start()
        return 0

    lax.fori_loop(0, shards, finish, 0)
    for s in range(shards):
        leave(s).wait()


def flash(at, lambdas, q, kv, rows):
    queries = q.shape[0]
    shards = queries // rows
    out = (shards, rows // 64, OUT_ROWS, 128)
    hbm = pl.BlockSpec(memory_space=pl.ANY)
    smem = pl.BlockSpec(memory_space=pltpu.SMEM)

    def body(*refs):
        flash_kernel(rows, *refs)

    return pl.pallas_call(
        body,
        out_shape=jax.ShapeDtypeStruct(out, bf16),
        in_specs=[smem, smem, pl.BlockSpec(memory_space=pltpu.VMEM), hbm],
        out_specs=hbm,
        scratch_shapes=[
            pltpu.VMEM(kv.shape, bf16),
            pltpu.VMEM(out, bf16),
            pltpu.SemaphoreType.DMA((kv.shape[0] // K_STEP,)),
            pltpu.SemaphoreType.DMA((shards,)),
            pltpu.VMEM((MAPS, 8, queries), f32),
            pltpu.VMEM((MAPS, HEAD_V + STAT, queries), f32),
            pltpu.VMEM((MAPS, 4 * HEAD_QK, queries), bf16),
            pltpu.VMEM((MAPS, K_STEP, Q_STEP), f32),
            pltpu.VMEM((MAPS, K_STEP, Q_STEP), f32),
            pltpu.VMEM((MAPS, 8, Q_STEP), f32),
            pltpu.VMEM((MAPS, 8, Q_STEP), f32),
        ],
        name="flash",
    )(at, lambdas, q, kv)


def merge_kernel(ways, tp, gain, *refs):
    sources, (out_ref, parts, conv, w), sems = refs[: 2 + ways], refs[2 + ways : -1], refs[-1]
    depth = w.shape[0] // ways
    held = [parts, conv] + [w.at[pl.ds(k * depth, depth)] for k in range(ways)]
    copies = [
        pltpu.make_async_copy(src, dst, sems.at[i])
        for i, (src, dst) in enumerate(zip(sources, held))
    ]
    for copy in copies:
        copy.start()
    copies[0].wait()
    count, _, _, lanes = parts.shape
    half = lanes // 2
    blocks = []
    for k in range(ways):
        h = (tp[0] + ways - k) % ways
        logs = []
        for d in range(count):
            stat = parts[d, h, HEAD_V:, :].astype(f32)
            logs.append(stat[0:1] + stat[1:2] + stat[2:3])
        peak = logs[0]
        for d in range(1, count):
            peak = jnp.maximum(peak, logs[d])
        weights = [jnp.exp2(x - peak) for x in logs]
        inverse = 1.0 / sum(weights)
        total = jnp.zeros((HEAD_V, lanes), f32)
        for d in range(count):
            total += parts[d, h, :HEAD_V, :].astype(f32) * (weights[d] * inverse)
        diff = total - pltpu.roll(total, half, 1)
        square = jnp.mean(diff * diff, axis=0, keepdims=True)
        heads = (diff * lax.rsqrt(square + 1e-6)).T * (gain[...] * 0.8)
        blocks.append(jnp.where(tp[0] % 2 == 1, heads[half:], heads[:half]).astype(bf16))
    heads = jnp.concatenate(blocks, axis=1)
    for copy in copies[1:]:
        copy.wait()
    out_ref[...] = (
        lax.dot_general(heads, w[...], NN, preferred_element_type=f32) + conv[...]
    ).astype(bf16)


def merge(tp, head_gain, parts, conv, weights):
    ways = len(weights)
    depth, width = weights[0].shape

    def body(*refs):
        merge_kernel(ways, *refs)

    return pl.pallas_call(
        body,
        out_shape=jax.ShapeDtypeStruct(conv.shape, bf16),
        in_specs=[pl.BlockSpec(memory_space=pltpu.SMEM), pl.BlockSpec(memory_space=pltpu.VMEM)]
        + [pl.BlockSpec(memory_space=pl.ANY)] * (2 + ways),
        out_specs=pl.BlockSpec(memory_space=pltpu.VMEM),
        scratch_shapes=[
            pltpu.VMEM(parts.shape, bf16),
            pltpu.VMEM(conv.shape, f32),
            pltpu.VMEM((ways * depth, width), bf16),
            pltpu.SemaphoreType.DMA((2 + ways,)),
        ],
        name="merge",
    )(tp, head_gain[None, :], parts, conv, *weights)


def halo(conv_mix, conv_input):
    count = lax.axis_size("sp")
    gated_in = (conv_mix.astype(f32) * conv_input.astype(f32)).astype(bf16)
    return lax.ppermute(gated_in[-2:], "sp", [(s, s + 1) for s in range(count - 1)])


def conv_branch(before, conv_gate, conv_mix, conv_input, conv_taps):
    gated_in = (conv_mix.astype(f32) * conv_input.astype(f32)).astype(bf16)
    extended = jnp.concatenate([before, gated_in], axis=0).astype(f32)
    taps = conv_taps.astype(f32)
    convolved = taps[0] * extended[:-2] + taps[1] * extended[1:-1] + taps[2] * extended[2:]
    return (conv_gate.astype(f32) * convolved).astype(bf16)


def layer(
    conv_gate,
    conv_mix,
    conv_input,
    conv_taps,
    query_rows,
    key_rows,
    value_rows,
    lambdas,
    head_gain,
    w_out_conv,
    w_out_heads,
):
    rows = query_rows.shape[0]
    count = lax.axis_size("sp")
    lines = count // (PLANES * CORES)
    own = lax.axis_index("sp")
    in_plane = lines * CORES
    z = own // in_plane
    at = jnp.stack([z // 2, z % 2, own % in_plane // CORES, own % CORES]).astype(jnp.int32)

    def place(p, e, x, c):
        return ((2 * p + e) * lines + x) * CORES + c

    peers = [
        [place(p, e, x, c) for e in range(2) for x in range(lines)]
        for p in range(PLANES // 2)
        for c in range(CORES)
    ]
    column = [
        [place(p, e, x, c) for p in range(PLANES // 2) for c in range(CORES)]
        for e in range(2)
        for x in range(lines)
    ]
    ways = lax.axis_size("tp")
    peers_by_head = [[member * ways + y for member in group for y in range(ways)] for group in peers]
    ways = lax.axis_size("tp")
    peers_by_head = [[member * ways + y for member in group for y in range(ways)] for group in peers]
    pair, copies = pack(query_rows, key_rows, value_rows, 2 * lines)
    keys = lax.all_gather(pair, "sp", axis=0, tiled=True, axis_index_groups=column)
    queries = lax.all_to_all(
        copies, "sp", split_axis=0, concat_axis=0, tiled=True, axis_index_groups=peers
    ).reshape(2 * lines * rows, -1)

    def moved(value, k):
        return lax.ppermute(value, "tp", [(y, (y + k) % ways) for y in range(ways)])

    before = halo(conv_mix, conv_input)
    weights = [w_out_heads]
    for k in range(1, ways):
        weights.append(moved(w_out_heads, k))
    conv_out = conv_branch(before, conv_gate, conv_mix, conv_input, conv_taps)
    conv_part = jnp.dot(conv_out, w_out_conv, preferred_element_type=f32).astype(bf16)
    conv_part = conv_part.reshape(ways, rows // ways, -1)
    own_y = lax.axis_index("tp")
    conv_sum = jnp.zeros(conv_part.shape[1:], f32)
    for k in range(ways):
        piece = lax.dynamic_index_in_dim(conv_part, (own_y + k) % ways, 0, keepdims=False)
        if k == ways - 1:
            piece, queries = lax.optimization_barrier((piece, queries))
        if k:
            piece = moved(piece, k)
        conv_sum += piece.astype(f32)
    keys, weights, conv_sum = lax.optimization_barrier((keys, weights, conv_sum))
    parts = flash(at, lambdas, queries, keys, rows)
    arrived = lax.all_to_all(
        parts.reshape(2 * lines * ways, OUT_ROWS, 128),
        ("sp", "tp"),
        split_axis=0,
        concat_axis=0,
        tiled=True,
        axis_index_groups=peers_by_head,
    ).reshape(2 * lines, ways, OUT_ROWS, 128)
    return merge(own_y.astype(jnp.int32)[None], head_gain, arrived, conv_sum, weights)


def solution(mesh):
    placed = (
        P("sp", "tp"),
        P("sp", "tp"),
        P("sp", "tp"),
        P(None, "tp"),
        P("sp", "tp"),
        P("sp", "tp"),
        P("sp", "tp"),
        P("tp"),
        P(),
        P("tp", None),
        P("tp", None),
    )
    return jax.shard_map(
        layer, mesh=mesh, in_specs=placed, out_specs=P(("sp", "tp"), None), check_vma=False
    )
```

profile of v0, /device:TPU:480, one launch (start us, length us, event | category | flops | bytes accessed | tf_op | source)
XLA Modules:
  0.0 121.0 jit_solution(15768474767507849541)
XLA Ops:
  6.5 1.9 %pack.1 = (bf16[256,256]{1,0:T(8,128)(2,1)}, bf16[8,256,128]{2,1,0:T(8,128)(2,1)}) custom-call(bf16[256,128]{1,0:T(8,128)(2,1)} %q_ref.1, bf16[256,128]{1,0:T(8,128)(2,1)} %k_ref.1, bf16[256,128]{1,0:T(8,128)(2,1)} %v_ref.1), custom_call_target="tpu_custom_call" | custom-call | tf_op jit(solution)/shard_map/pack/pallas_call | solution.py:36
  8.4 0.0 all-gather.2.cloned.1.call-update
  8.4 5.8 %all-to-all-start = ((bf16[8,256,128]{2,1,0:T(8,128)(2,1)}), bf16[8,256,128]{2,1,0:T(8,128)(2,1)S(1)}, u32[]{:S(2)}, u32[]{:S(2)}) async-start(bf16[8,256,128]{2,1,0:T(8,128)(2,1)} %get-tuple-element.15), calls=%async_computation | async-start | bytes 1048576 | tf_op jit(solution)/shard_map/all_to_all | solution.py:330
  14.2 0.9 multiply_convert_fusion
  15.2 1.9 %collective-permute-start = (bf16[2,128]{1,0:T(2,128)(2,1)S(1)}, bf16[2,128]{1,0:T(2,128)(2,1)S(1)}, u32[]{:S(2)}, u32[]{:S(2)}) collective-permute-start(bf16[2,128]{1,0:T(2,128)(2,1)S(1)} %slice.28), channel_id=1, source_target_pairs={{0,4},{4,8},{8,12},{12,16},{16,20},{20,24},{24,28},{28,32},{32,36}... | collective-permute-start | bytes 1544 | tf_op jit(solution)/shard_map/ppermute | solution.py:279
  17.1 0.7 convert_element_type.43
  17.8 4.6 %collective-permute-done = bf16[2,128]{1,0:T(2,128)(2,1)S(1)} collective-permute-done((bf16[2,128]{1,0:T(2,128)(2,1)S(1)}, bf16[2,128]{1,0:T(2,128)(2,1)S(1)}, u32[]{:S(2)}, u32[]{:S(2)}) %collective-permute-start) | collective-permute-done | bytes 544 | tf_op jit(solution)/shard_map/ppermute | solution.py:279
  22.4 1.3 %convolution_convert_fusion = bf16[256,2048]{1,0:T(8,128)(2,1)S(1)} fusion(bf16[128,2048]{1,0:T(8,128)(2,1)S(1)} %copy-done, f32[258,128]{1,0:T(8,128)S(1)} %maximum_convert_fusion, bf16[256,128]{1,0:T(8,128)(2,1)} %param.11, f32[128]{0:T(128)S(1)} %get-tuple-element.29, f32[128]{0:T(128)S(1)} %get-tuple-element.30, f32[128]{0:T(128)S(1)} %get-tuple-element.28), kind=kOutput, calls=%fused_computation | convolution fusion | flops 135004160 | bytes 2033152 | tf_op jit(solution)/shard_map/dot_general | solution.py:342
  23.7 0.9 dynamic-slice_bitcast_fusion.1
  24.6 3.5 %collective-permute-start.4 = (bf16[64,2048]{1,0:T(8,128)(2,1)}, bf16[64,2048]{1,0:T(8,128)(2,1)}, u32[]{:S(2)}, u32[]{:S(2)}) collective-permute-start(bf16[64,2048]{1,0:T(8,128)(2,1)} %get-tuple-element.25), channel_id=1, source_target_pairs={{0,1},{1,2},{2,3},{3,0},{4,5},{5,6},{6,7},{7,4},{8,9},{9,10},{10,1... | collective-permute-start | bytes 786440 | tf_op jit(solution)/shard_map/ppermute | solution.py:335
  28.1 4.8 %collective-permute-start.5 = (bf16[64,2048]{1,0:T(8,128)(2,1)}, bf16[64,2048]{1,0:T(8,128)(2,1)}, u32[]{:S(2)}, u32[]{:S(2)}) collective-permute-start(bf16[64,2048]{1,0:T(8,128)(2,1)} %get-tuple-element.26), channel_id=1, source_target_pairs={{0,2},{1,3},{2,0},{3,1},{4,6},{5,7},{6,4},{7,5},{8,10},{9,11},{10,... | collective-permute-start | bytes 786440 | tf_op jit(solution)/shard_map/ppermute | solution.py:335
  32.9 0.0 all-to-all-done
  32.9 3.3 %collective-permute-start.6 = (bf16[64,2048]{1,0:T(8,128)(2,1)S(1)}, bf16[64,2048]{1,0:T(8,128)(2,1)}, u32[]{:S(2)}, u32[]{:S(2)}) collective-permute-start(bf16[64,2048]{1,0:T(8,128)(2,1)S(1)} %get-tuple-element.18), channel_id=1, source_target_pairs={{0,3},{1,0},{2,1},{3,2},{4,7},{5,4},{6,5},{7,6},{8,11},{9,8},{10,9... | collective-permute-start | bytes 786440 | tf_op jit(solution)/shard_map/ppermute | solution.py:335
  36.2 2.6 %collective-permute-start.1 = (bf16[128,2048]{1,0:T(8,128)(2,1)S(1)}, bf16[128,2048]{1,0:T(8,128)(2,1)S(1)}, u32[]{:S(2)}, u32[]{:S(2)}) collective-permute-start(bf16[128,2048]{1,0:T(8,128)(2,1)S(1)} %copy-done.2), channel_id=1, source_target_pairs={{0,1},{1,2},{2,3},{3,0},{4,5},{5,6},{6,7},{7,4},{8,9},{9,10},{10,1... | collective-permute-start | bytes 1572872 | tf_op jit(solution)/shard_map/ppermute | solution.py:335
  38.8 2.7 %collective-permute-start.2 = (bf16[128,2048]{1,0:T(8,128)(2,1)S(1)}, bf16[128,2048]{1,0:T(8,128)(2,1)}, u32[]{:S(2)}, u32[]{:S(2)}) collective-permute-start(bf16[128,2048]{1,0:T(8,128)(2,1)S(1)} %copy-done.2), channel_id=1, source_target_pairs={{0,2},{1,3},{2,0},{3,1},{4,6},{5,7},{6,4},{7,5},{8,10},{9,11},{10,... | collective-permute-start | bytes 1572872 | tf_op jit(solution)/shard_map/ppermute | solution.py:335
  41.6 3.8 %collective-permute-start.3 = (bf16[128,2048]{1,0:T(8,128)(2,1)S(1)}, bf16[128,2048]{1,0:T(8,128)(2,1)}, u32[]{:S(2)}, u32[]{:S(2)}) collective-permute-start(bf16[128,2048]{1,0:T(8,128)(2,1)S(1)} %copy-done.2), channel_id=1, source_target_pairs={{0,3},{1,0},{2,1},{3,2},{4,7},{5,4},{6,5},{7,6},{8,11},{9,8},{10,9... | collective-permute-start | bytes 1572872 | tf_op jit(solution)/shard_map/ppermute | solution.py:335
  45.4 0.6 pad_add_fusion.refs_0_
  46.6 3.1 %collective-permute-done.6 = bf16[64,2048]{1,0:T(8,128)(2,1)} collective-permute-done((bf16[64,2048]{1,0:T(8,128)(2,1)S(1)}, bf16[64,2048]{1,0:T(8,128)(2,1)}, u32[]{:S(2)}, u32[]{:S(2)}) %collective-permute-start.6) | collective-permute-done | bytes 262176 | tf_op jit(solution)/shard_map/ppermute | solution.py:335
  49.8 2.0 %fusion.1.refs_3_ = f32[64,2048]{1,0:T(8,128)} fusion(bf16[64,2048]{1,0:T(8,128)(2,1)} %collective-permute-done.6, bf16[64,2048]{1,0:T(8,128)(2,1)} %collective-permute-done.5, bf16[64,2048]{1,0:T(8,128)(2,1)} %collective-permute-done.4, bf16[4,64,2048]{2,1,0:T(8,128)(2,1)S(1)} %bitcast.29, s32[]{:T(128)S(6)} %select_n.63), kind=kLoop, calls=%fused_computation.3 | loop fusion | flops 917504 | bytes 1572868 | tf_op jit(solution)/shard_map/add | solution.py:352
  51.8 11.4 %collective-permute-done.1.refs_5_ = bf16[128,2048]{1,0:T(8,128)(2,1)S(1)} collective-permute-done((bf16[128,2048]{1,0:T(8,128)(2,1)S(1)}, bf16[128,2048]{1,0:T(8,128)(2,1)S(1)}, u32[]{:S(2)}, u32[]{:S(2)}) %collective-permute-start.1) | collective-permute-done | bytes 524320 | tf_op jit(solution)/shard_map/ppermute | solution.py:335
  63.2 1.6 %collective-permute-done.3.refs_7_ = bf16[128,2048]{1,0:T(8,128)(2,1)} collective-permute-done((bf16[128,2048]{1,0:T(8,128)(2,1)S(1)}, bf16[128,2048]{1,0:T(8,128)(2,1)}, u32[]{:S(2)}, u32[]{:S(2)}) %collective-permute-start.3) | collective-permute-done | bytes 524320 | tf_op jit(solution)/shard_map/ppermute | solution.py:335
  64.8 21.0 %flash.1 = bf16[8,4,136,128]{3,2,1,0:T(8,128)(2,1)} custom-call(s32[4]{0:T(128)} %pad_add_fusion.refs_0_, f32[1]{0:T(128)S(6)} %copy.12.refs_1_, bf16[2048,128]{1,0:T(8,128)(2,1)} %bitcast.30, bf16[4096,256]{1,0:T(8,128)(2,1)} %all-gather.2.cloned.1.call-done.refs_3_), custom_call_target="tpu_custom_call" | custom-call | tf_op jit(solution)/shard_map/flash/pallas_call | solution.py:191
  85.8 24.4 %all_to_all.10 = bf16[32,136,128]{2,1,0:T(8,128)(2,1)} all-to-all(bf16[32,136,128]{2,1,0:T(8,128)(2,1)} %bitcast.27), channel_id=1, replica_groups={{0,1,2,3,8,9,10,11,16,17,18,19,24,25,26,27,32,33,34,35,40,41,42,43,48,4..., dimensions={0} | all-to-all | bytes 2228224 | tf_op jit(solution)/shard_map/all_to_all | solution.py:355
  110.2 3.9 %merge.1 = bf16[64,2048]{1,0:T(8,128)(2,1)} custom-call(s32[1]{0:T(128)} %bitcast.refs_0_, f32[1,128]{1,0:T(1,128)} %bitcast.31, bf16[8,4,136,128]{3,2,1,0:T(8,128)(2,1)} %bitcast.26, f32[64,2048]{1,0:T(8,128)} %fusion.1.refs_3_, bf16[128,2048]{1,0:T(8,128)(2,1)} %refs_4_, bf16[128,2048]{1,0:T(8,128)(2,1)} %copy-done.3, ...), custom_call_target="tpu_custom_call" | custom-call | tf_op jit(solution)/shard_map/merge/pallas_call | solution.py:260
  (16 shorter events, 0.1 us)
Async XLA Ops:
  6.5 15.9 %copy-start = (bf16[128,2048]{1,0:T(8,128)(2,1)S(1)}, bf16[128,2048]{1,0:T(8,128)(2,1)}, u32[]{:S(2)}) copy-start(bf16[128,2048]{1,0:T(8,128)(2,1)} %param.20) | copy-start | bytes 1572868
  6.5 58.3 %all-gather.2.cloned.1.call-start = ((), (), s32[]{:S(2)}) async-start(), calls=%async_computation.2 | async-start | bytes 2228224 | tf_op jit(solution)/shard_map/all_gather | solution.py:329
  8.4 24.5 %all-to-all-start = ((bf16[8,256,128]{2,1,0:T(8,128)(2,1)}), bf16[8,256,128]{2,1,0:T(8,128)(2,1)S(1)}, u32[]{:S(2)}, u32[]{:S(2)}) async-start(bf16[8,256,128]{2,1,0:T(8,128)(2,1)} %get-tuple-element.15), calls=%async_computation | async-start | bytes 1048576 | tf_op jit(solution)/shard_map/all_to_all | solution.py:330
  14.2 22.0 %copy-start.2 = (bf16[128,2048]{1,0:T(8,128)(2,1)S(1)}, bf16[128,2048]{1,0:T(8,128)(2,1)}, u32[]{:S(2)}) copy-start(bf16[128,2048]{1,0:T(8,128)(2,1)} %refs_4_) | copy-start | bytes 1572868
  15.2 7.2 %collective-permute-start = (bf16[2,128]{1,0:T(2,128)(2,1)S(1)}, bf16[2,128]{1,0:T(2,128)(2,1)S(1)}, u32[]{:S(2)}, u32[]{:S(2)}) collective-permute-start(bf16[2,128]{1,0:T(2,128)(2,1)S(1)} %slice.28), channel_id=1, source_target_pairs={{0,4},{4,8},{8,12},{12,16},{16,20},{20,24},{24,28},{28,32},{32,36}... | collective-permute-start | bytes 1544 | tf_op jit(solution)/shard_map/ppermute | solution.py:279
  24.6 17.0 %collective-permute-start.4 = (bf16[64,2048]{1,0:T(8,128)(2,1)}, bf16[64,2048]{1,0:T(8,128)(2,1)}, u32[]{:S(2)}, u32[]{:S(2)}) collective-permute-start(bf16[64,2048]{1,0:T(8,128)(2,1)} %get-tuple-element.25), channel_id=1, source_target_pairs={{0,1},{1,2},{2,3},{3,0},{4,5},{5,6},{6,7},{7,4},{8,9},{9,10},{10,1... | collective-permute-start | bytes 786440 | tf_op jit(solution)/shard_map/ppermute | solution.py:335
  28.1 18.6 %collective-permute-start.5 = (bf16[64,2048]{1,0:T(8,128)(2,1)}, bf16[64,2048]{1,0:T(8,128)(2,1)}, u32[]{:S(2)}, u32[]{:S(2)}) collective-permute-start(bf16[64,2048]{1,0:T(8,128)(2,1)} %get-tuple-element.26), channel_id=1, source_target_pairs={{0,2},{1,3},{2,0},{3,1},{4,6},{5,7},{6,4},{7,5},{8,10},{9,11},{10,... | collective-permute-start | bytes 786440 | tf_op jit(solution)/shard_map/ppermute | solution.py:335
  32.9 31.9 %copy-start.1 = (bf16[8,256,128]{2,1,0:T(8,128)(2,1)}, bf16[8,256,128]{2,1,0:T(8,128)(2,1)S(1)}, u32[]{:S(2)}) copy-start(bf16[8,256,128]{2,1,0:T(8,128)(2,1)S(1)} %all-to-all-done) | copy-start | bytes 1572868
  32.9 16.8 %collective-permute-start.6 = (bf16[64,2048]{1,0:T(8,128)(2,1)S(1)}, bf16[64,2048]{1,0:T(8,128)(2,1)}, u32[]{:S(2)}, u32[]{:S(2)}) collective-permute-start(bf16[64,2048]{1,0:T(8,128)(2,1)S(1)} %get-tuple-element.18), channel_id=1, source_target_pairs={{0,3},{1,0},{2,1},{3,2},{4,7},{5,4},{6,5},{7,6},{8,11},{9,8},{10,9... | collective-permute-start | bytes 786440 | tf_op jit(solution)/shard_map/ppermute | solution.py:335
  36.2 27.0 %collective-permute-start.1 = (bf16[128,2048]{1,0:T(8,128)(2,1)S(1)}, bf16[128,2048]{1,0:T(8,128)(2,1)S(1)}, u32[]{:S(2)}, u32[]{:S(2)}) collective-permute-start(bf16[128,2048]{1,0:T(8,128)(2,1)S(1)} %copy-done.2), channel_id=1, source_target_pairs={{0,1},{1,2},{2,3},{3,0},{4,5},{5,6},{6,7},{7,4},{8,9},{9,10},{10,1... | collective-permute-start | bytes 1572872 | tf_op jit(solution)/shard_map/ppermute | solution.py:335
  38.8 24.4 %collective-permute-start.2 = (bf16[128,2048]{1,0:T(8,128)(2,1)S(1)}, bf16[128,2048]{1,0:T(8,128)(2,1)}, u32[]{:S(2)}, u32[]{:S(2)}) collective-permute-start(bf16[128,2048]{1,0:T(8,128)(2,1)S(1)} %copy-done.2), channel_id=1, source_target_pairs={{0,2},{1,3},{2,0},{3,1},{4,6},{5,7},{6,4},{7,5},{8,10},{9,11},{10,... | collective-permute-start | bytes 1572872 | tf_op jit(solution)/shard_map/ppermute | solution.py:335
  41.6 23.2 %collective-permute-start.3 = (bf16[128,2048]{1,0:T(8,128)(2,1)S(1)}, bf16[128,2048]{1,0:T(8,128)(2,1)}, u32[]{:S(2)}, u32[]{:S(2)}) collective-permute-start(bf16[128,2048]{1,0:T(8,128)(2,1)S(1)} %copy-done.2), channel_id=1, source_target_pairs={{0,3},{1,0},{2,1},{3,2},{4,7},{5,4},{6,5},{7,6},{8,11},{9,8},{10,9... | collective-permute-start | bytes 1572872 | tf_op jit(solution)/shard_map/ppermute | solution.py:335
  63.2 47.0 %copy-start.3 = (bf16[128,2048]{1,0:T(8,128)(2,1)}, bf16[128,2048]{1,0:T(8,128)(2,1)S(1)}, u32[]{:S(2)}) copy-start(bf16[128,2048]{1,0:T(8,128)(2,1)S(1)} %collective-permute-done.1.refs_5_) | copy-start | bytes 1572868
Sparse Core Ops, SparseCore 0:
  9.4 51.3 all-gather.1
where the time goes:
time: 122 us; the launch traced here: 121 us
  starting transfers between devices  28.3 us (23%)
  Pallas kernels  26.7 us (22%)
  blocking collectives  24.4 us (20%)
  waiting for transfers between devices  20.8 us (17%)
  between operations  14.3 us (12%)
  other arithmetic  4.27 us (3%)
  matrix products  1.26 us (1%)
    all_to_all x1, blocking collectives, layer(): lax.all_to_all(parts.reshape(2 * lines * ways, OUT_ROWS, 128), ('sp', 'tp...  24.4 us
    pallas_call x1, Pallas kernels, flash(): pl.pallas_call(body, out_shape=jax.ShapeDtypeStruct(out, bf16), in_specs=...  21 us
    ppermute x6, starting transfers between devices, moved(): return lax.ppermute(value, 'tp', [(y, (y + k) % ways) for y in range(ways)])  20.6 us
    ppermute x6, waiting for transfers between devices, moved(): return lax.ppermute(value, 'tp', [(y, (y + k) % ways) for y in range(ways)])  16.2 us
    all_to_all x1, starting transfers between devices, layer(): lax.all_to_all(copies, 'sp', split_axis=0, concat_axis=0, tiled=True, axi...  5.77 us
    ppermute x1, waiting for transfers between devices, halo(): lax.ppermute(gated_in[-2:], 'sp', [(s, s + 1) for s in range(count - 1)])  4.58 us
    pallas_call x1, Pallas kernels, merge(): pl.pallas_call(body, out_shape=jax.ShapeDtypeStruct(conv.shape, bf16), in...  3.9 us
  transfers between devices with their start and end apart: 9, of which 4 were waited for; matrix products, arithmetic and copies ran while one was open for 5% of the time, Pallas kernels for 0%

commit v1 on v0

--- a/solution.py
+++ b/solution.py
@@ -342,16 +342,18 @@
     conv_part = jnp.dot(conv_out, w_out_conv, preferred_element_type=f32).astype(bf16)
     conv_part = conv_part.reshape(ways, rows // ways, -1)
     own_y = lax.axis_index("tp")
-    conv_sum = jnp.zeros(conv_part.shape[1:], f32)
+    pieces = []
     for k in range(ways):
         piece = lax.dynamic_index_in_dim(conv_part, (own_y + k) % ways, 0, keepdims=False)
         if k == ways - 1:
             piece, queries = lax.optimization_barrier((piece, queries))
         if k:
             piece = moved(piece, k)
-        conv_sum += piece.astype(f32)
-    keys, weights, conv_sum = lax.optimization_barrier((keys, weights, conv_sum))
+        pieces.append(piece)
+    keys, weights, pieces = lax.optimization_barrier((keys, weights, pieces))
     parts = flash(at, lambdas, queries, keys, rows)
+    parts, pieces = lax.optimization_barrier((parts, pieces))
+    conv_sum = sum(piece.astype(f32) for piece in pieces)
     arrived = lax.all_to_all(
         parts.reshape(2 * lines * ways, OUT_ROWS, 128),
         ("sp", "tp"),

time: 122 us -> 119 us (0.975)
  blocking collectives: 24.4 us -> 0 us
  starting transfers between devices: 28.3 us -> 41.2 us
  waiting for transfers between devices: 20.8 us -> 28.2 us
    all_to_all x1 -> x0, blocking collectives: 24.4 us -> none  [layer(): lax.all_to_all(parts.reshape(2 * lines * ways, OUT_ROWS, 128), ('sp', 'tp...]
    all_to_all x0 -> x1, waiting for transfers between devices: none -> 15.1 us  [layer(): lax.all_to_all(parts.reshape(2 * lines * ways, OUT_ROWS, 128), ('sp', 'tp...]
    all_to_all x0 -> x1, starting transfers between devices: none -> 9.97 us  [layer(): lax.all_to_all(parts.reshape(2 * lines * ways, OUT_ROWS, 128), ('sp', 'tp...]
    ppermute x1, waiting for transfers between devices: 4.58 us -> 0.01 us  [halo(): lax.ppermute(gated_in[-2:], 'sp', [(s, s + 1) for s in range(count - 1)])]
    ppermute x6, waiting for transfers between devices: 16.2 us -> 13 us  [moved(): return lax.ppermute(value, 'tp', [(y, (y + k) % ways) for y in range(ways)])]
    ppermute x6, starting transfers between devices: 20.6 us -> 23.5 us  [moved(): return lax.ppermute(value, 'tp', [(y, (y + k) % ways) for y in range(ways)])]
  transfers between devices with their start and end apart: 9 -> 10, of which waited for: 4 -> 3; matrix products, arithmetic and copies ran while one was open for 5% -> 5% of each run, Pallas kernels for 0% -> 0%
where the time goes in v1:
time: 119 us; the launch traced here: 118 us
  starting transfers between devices  41.2 us (35%)
  waiting for transfers between devices  28.2 us (24%)
  Pallas kernels  27.1 us (23%)
  between operations  14.4 us (12%)
  other arithmetic  4.3 us (4%)
  local copies, waits for them, and re-layouts  1.99 us (2%)
  matrix products  1.26 us (1%)
    ppermute x6, starting transfers between devices, moved(): return lax.ppermute(value, 'tp', [(y, (y + k) % ways) for y in range(ways)])  23.5 us
    pallas_call x1, Pallas kernels, flash(): pl.pallas_call(body, out_shape=jax.ShapeDtypeStruct(out, bf16), in_specs=...  21.4 us
    all_to_all x1, waiting for transfers between devices, layer(): lax.all_to_all(parts.reshape(2 * lines * ways, OUT_ROWS, 128), ('sp', 'tp...  15.1 us
    ppermute x6, waiting for transfers between devices, moved(): return lax.ppermute(value, 'tp', [(y, (y + k) % ways) for y in range(ways)])  13 us
    all_to_all x1, starting transfers between devices, layer(): lax.all_to_all(parts.reshape(2 * lines * ways, OUT_ROWS, 128), ('sp', 'tp...  9.97 us
    all_to_all x1, starting transfers between devices, layer(): lax.all_to_all(copies, 'sp', split_axis=0, concat_axis=0, tiled=True, axi...  5.77 us
    pallas_call x1, Pallas kernels, merge(): pl.pallas_call(body, out_shape=jax.ShapeDtypeStruct(conv.shape, bf16), in...  3.9 us
  transfers between devices with their start and end apart: 10, of which 3 were waited for; matrix products, arithmetic and copies ran while one was open for 5% of the time, Pallas kernels for 0%

profile of v1, /device:TPU:480, one launch (start us, length us, event | category | flops | bytes accessed | tf_op | source)
XLA Modules:
  0.0 118.4 jit_solution(6906710274580125970)
XLA Ops:
  6.5 1.8 %pack.1 = (bf16[256,256]{1,0:T(8,128)(2,1)}, bf16[8,256,128]{2,1,0:T(8,128)(2,1)}) custom-call(bf16[256,128]{1,0:T(8,128)(2,1)} %q_ref.1, bf16[256,128]{1,0:T(8,128)(2,1)} %k_ref.1, bf16[256,128]{1,0:T(8,128)(2,1)} %v_ref.1), custom_call_target="tpu_custom_call" | custom-call | tf_op jit(solution)/shard_map/pack/pallas_call | solution.py:36
  8.4 0.0 all-gather.2.cloned.1.call-update
  8.4 5.8 %all-to-all-start = ((bf16[8,256,128]{2,1,0:T(8,128)(2,1)}), bf16[8,256,128]{2,1,0:T(8,128)(2,1)S(1)}, u32[]{:S(2)}, u32[]{:S(2)}) async-start(bf16[8,256,128]{2,1,0:T(8,128)(2,1)} %get-tuple-element.23), calls=%async_computation | async-start | bytes 1048576 | tf_op jit(solution)/shard_map/all_to_all | solution.py:330
  14.2 0.9 multiply_convert_fusion
  15.1 1.9 %collective-permute-start = (bf16[2,128]{1,0:T(2,128)(2,1)S(1)}, bf16[2,128]{1,0:T(2,128)(2,1)S(1)}, u32[]{:S(2)}, u32[]{:S(2)}) collective-permute-start(bf16[2,128]{1,0:T(2,128)(2,1)S(1)} %slice.28), channel_id=1, source_target_pairs={{0,4},{4,8},{8,12},{12,16},{16,20},{20,24},{24,28},{28,32},{32,36}... | collective-permute-start | bytes 1544 | tf_op jit(solution)/shard_map/ppermute | solution.py:279
  17.0 5.1 %collective-permute-start.2 = (bf16[128,2048]{1,0:T(8,128)(2,1)}, bf16[128,2048]{1,0:T(8,128)(2,1)S(1)}, u32[]{:S(2)}, u32[]{:S(2)}) collective-permute-start(bf16[128,2048]{1,0:T(8,128)(2,1)} %refs_4_), channel_id=1, source_target_pairs={{0,2},{1,3},{2,0},{3,1},{4,6},{5,7},{6,4},{7,5},{8,10},{9,11},{10,... | collective-permute-start | bytes 1572872 | tf_op jit(solution)/shard_map/ppermute | solution.py:335
  22.2 0.7 convert_element_type.40
  22.9 1.3 %convolution_convert_fusion = bf16[256,2048]{1,0:T(8,128)(2,1)S(1)} fusion(bf16[128,2048]{1,0:T(8,128)(2,1)S(1)} %copy-done, f32[258,128]{1,0:T(8,128)S(1)} %maximum_convert_fusion, bf16[256,128]{1,0:T(8,128)(2,1)} %param.11, f32[128]{0:T(128)S(1)} %get-tuple-element.46, f32[128]{0:T(128)S(1)} %get-tuple-element.47, f32[128]{0:T(128)S(1)} %get-tuple-element.45), kind=kOutput, calls=%fused_computation | convolution fusion | flops 135004160 | bytes 2033152 | tf_op jit(solution)/shard_map/dot_general | solution.py:342
  24.2 0.9 dynamic-slice_bitcast_fusion
  25.1 4.5 %collective-permute-start.5 = (bf16[64,2048]{1,0:T(8,128)(2,1)}, bf16[64,2048]{1,0:T(8,128)(2,1)}, u32[]{:S(2)}, u32[]{:S(2)}) collective-permute-start(bf16[64,2048]{1,0:T(8,128)(2,1)} %get-tuple-element.41), channel_id=1, source_target_pairs={{0,2},{1,3},{2,0},{3,1},{4,6},{5,7},{6,4},{7,5},{8,10},{9,11},{10,... | collective-permute-start | bytes 786440 | tf_op jit(solution)/shard_map/ppermute | solution.py:335
  29.7 2.6 %collective-permute-start.1 = (bf16[128,2048]{1,0:T(8,128)(2,1)S(1)}, bf16[128,2048]{1,0:T(8,128)(2,1)S(1)}, u32[]{:S(2)}, u32[]{:S(2)}) collective-permute-start(bf16[128,2048]{1,0:T(8,128)(2,1)S(1)} %copy-done.3), channel_id=1, source_target_pairs={{0,1},{1,2},{2,3},{3,0},{4,5},{5,6},{6,7},{7,4},{8,9},{9,10},{10,1... | collective-permute-start | bytes 1572872 | tf_op jit(solution)/shard_map/ppermute | solution.py:335
  32.3 4.5 %collective-permute-start.3 = (bf16[128,2048]{1,0:T(8,128)(2,1)S(1)}, bf16[128,2048]{1,0:T(8,128)(2,1)S(1)}, u32[]{:S(2)}, u32[]{:S(2)}) collective-permute-start(bf16[128,2048]{1,0:T(8,128)(2,1)S(1)} %copy-done.3), channel_id=1, source_target_pairs={{0,3},{1,0},{2,1},{3,2},{4,7},{5,4},{6,5},{7,6},{8,11},{9,8},{10,9... | collective-permute-start | bytes 1572872 | tf_op jit(solution)/shard_map/ppermute | solution.py:335
  36.8 1.9 %collective-permute-start.4 = (bf16[64,2048]{1,0:T(8,128)(2,1)}, bf16[64,2048]{1,0:T(8,128)(2,1)}, u32[]{:S(2)}, u32[]{:S(2)}) collective-permute-start(bf16[64,2048]{1,0:T(8,128)(2,1)} %get-tuple-element.42), channel_id=1, source_target_pairs={{0,1},{1,2},{2,3},{3,0},{4,5},{5,6},{6,7},{7,4},{8,9},{9,10},{10,1... | collective-permute-start | bytes 786440 | tf_op jit(solution)/shard_map/ppermute | solution.py:335
  38.7 1.9 %collective-permute-done.5 = bf16[64,2048]{1,0:T(8,128)(2,1)} collective-permute-done((bf16[64,2048]{1,0:T(8,128)(2,1)}, bf16[64,2048]{1,0:T(8,128)(2,1)}, u32[]{:S(2)}, u32[]{:S(2)}) %collective-permute-start.5) | collective-permute-done | bytes 262176 | tf_op jit(solution)/shard_map/ppermute | solution.py:335
  40.6 4.9 %collective-permute-start.6 = (bf16[64,2048]{1,0:T(8,128)(2,1)}, bf16[64,2048]{1,0:T(8,128)(2,1)}, u32[]{:S(2)}, u32[]{:S(2)}) collective-permute-start(bf16[64,2048]{1,0:T(8,128)(2,1)} %get-tuple-element.26), channel_id=1, source_target_pairs={{0,3},{1,0},{2,1},{3,2},{4,7},{5,4},{6,5},{7,6},{8,11},{9,8},{10,9... | collective-permute-start | bytes 786440 | tf_op jit(solution)/shard_map/ppermute | solution.py:335
  46.3 0.6 pad_add_fusion.refs_0_
  46.9 11.1 %collective-permute-done.4 = bf16[64,2048]{1,0:T(8,128)(2,1)} collective-permute-done((bf16[64,2048]{1,0:T(8,128)(2,1)}, bf16[64,2048]{1,0:T(8,128)(2,1)}, u32[]{:S(2)}, u32[]{:S(2)}) %collective-permute-start.4) | collective-permute-done | bytes 262176 | tf_op jit(solution)/shard_map/ppermute | solution.py:335
  58.0 0.0 all-gather.2.cloned.1.call-done.refs_3_
  58.1 21.4 %flash.1 = bf16[8,4,136,128]{3,2,1,0:T(8,128)(2,1)} custom-call(s32[4]{0:T(128)} %pad_add_fusion.refs_0_, f32[1]{0:T(128)S(6)} %copy.12.refs_1_, bf16[2048,128]{1,0:T(8,128)(2,1)} %bitcast.28, bf16[4096,256]{1,0:T(8,128)(2,1)} %all-gather.2.cloned.1.call-done.refs_3_), custom_call_target="tpu_custom_call" | custom-call | tf_op jit(solution)/shard_map/flash/pallas_call | solution.py:191
  79.5 10.0 %all-to-all-start.1 = ((bf16[32,136,128]{2,1,0:T(8,128)(2,1)}), bf16[32,136,128]{2,1,0:T(8,128)(2,1)S(1)}, u32[]{:S(2)}, u32[]{:S(2)}) async-start(bf16[32,136,128]{2,1,0:T(8,128)(2,1)} %bitcast.26), calls=%async_computation.1 | async-start | bytes 2228224 | tf_op jit(solution)/shard_map/all_to_all | solution.py:357
  89.5 2.0 %convert_add_fusion.refs_3_ = f32[64,2048]{1,0:T(8,128)} fusion(bf16[64,2048]{1,0:T(8,128)(2,1)} %collective-permute-done.6, bf16[64,2048]{1,0:T(8,128)(2,1)} %collective-permute-done.5, bf16[64,2048]{1,0:T(8,128)(2,1)} %collective-permute-done.4, bf16[64,2048]{1,0:T(8,128)(2,1)S(1)} %get-tuple-element.33), kind=kLoop, calls=%fused_computation.1 | loop fusion | flops 917504 | bytes 1572864 | tf_op jit(solution)/shard_map/add | solution.py:356
  91.5 15.1 %all-to-all-done.1 = bf16[32,136,128]{2,1,0:T(8,128)(2,1)S(1)} async-done(((bf16[32,136,128]{2,1,0:T(8,128)(2,1)}), bf16[32,136,128]{2,1,0:T(8,128)(2,1)S(1)}, u32[]{:S(2)}, u32[]{:S(2)}) %all-to-all-start.1) | async-done | bytes 1114144 | tf_op jit(solution)/shard_map/all_to_all | solution.py:357
  106.6 1.0 copy-done.1
  107.6 3.9 %merge.1 = bf16[64,2048]{1,0:T(8,128)(2,1)} custom-call(s32[1]{0:T(128)} %bitcast.refs_0_, f32[1,128]{1,0:T(1,128)} %bitcast.29, bf16[8,4,136,128]{3,2,1,0:T(8,128)(2,1)} %bitcast.25, f32[64,2048]{1,0:T(8,128)} %convert_add_fusion.refs_3_, bf16[128,2048]{1,0:T(8,128)(2,1)} %refs_4_, bf16[128,2048]{1,0:T(8,128)(2,1)} %copy-done.5, ...), custom_call_target="tpu_custom_call" | custom-call | tf_op jit(solution)/shard_map/merge/pallas_call | solution.py:260
  (23 shorter events, 0.1 us)
Async XLA Ops:
  6.5 16.4 %copy-start = (bf16[128,2048]{1,0:T(8,128)(2,1)S(1)}, bf16[128,2048]{1,0:T(8,128)(2,1)}, u32[]{:S(2)}) copy-start(bf16[128,2048]{1,0:T(8,128)(2,1)} %param.20) | copy-start | bytes 1572868
  6.5 51.5 %all-gather.2.cloned.1.call-start = ((), (), s32[]{:S(2)}) async-start(), calls=%async_computation.2 | async-start | bytes 2228224 | tf_op jit(solution)/shard_map/all_gather | solution.py:329
  8.4 30.3 %all-to-all-start = ((bf16[8,256,128]{2,1,0:T(8,128)(2,1)}), bf16[8,256,128]{2,1,0:T(8,128)(2,1)S(1)}, u32[]{:S(2)}, u32[]{:S(2)}) async-start(bf16[8,256,128]{2,1,0:T(8,128)(2,1)} %get-tuple-element.23), calls=%async_computation | async-start | bytes 1048576 | tf_op jit(solution)/shard_map/all_to_all | solution.py:330
  15.1 7.8 %collective-permute-start = (bf16[2,128]{1,0:T(2,128)(2,1)S(1)}, bf16[2,128]{1,0:T(2,128)(2,1)S(1)}, u32[]{:S(2)}, u32[]{:S(2)}) collective-permute-start(bf16[2,128]{1,0:T(2,128)(2,1)S(1)} %slice.28), channel_id=1, source_target_pairs={{0,4},{4,8},{8,12},{12,16},{16,20},{20,24},{24,28},{28,32},{32,36}... | collective-permute-start | bytes 1544 | tf_op jit(solution)/shard_map/ppermute | solution.py:279
  17.0 41.0 %collective-permute-start.2 = (bf16[128,2048]{1,0:T(8,128)(2,1)}, bf16[128,2048]{1,0:T(8,128)(2,1)S(1)}, u32[]{:S(2)}, u32[]{:S(2)}) collective-permute-start(bf16[128,2048]{1,0:T(8,128)(2,1)} %refs_4_), channel_id=1, source_target_pairs={{0,2},{1,3},{2,0},{3,1},{4,6},{5,7},{6,4},{7,5},{8,10},{9,11},{10,... | collective-permute-start | bytes 1572872 | tf_op jit(solution)/shard_map/ppermute | solution.py:335
  22.1 7.6 %copy-start.3 = (bf16[128,2048]{1,0:T(8,128)(2,1)S(1)}, bf16[128,2048]{1,0:T(8,128)(2,1)}, u32[]{:S(2)}) copy-start(bf16[128,2048]{1,0:T(8,128)(2,1)} %refs_4_) | copy-start | bytes 1572868
  25.1 15.5 %collective-permute-start.5 = (bf16[64,2048]{1,0:T(8,128)(2,1)}, bf16[64,2048]{1,0:T(8,128)(2,1)}, u32[]{:S(2)}, u32[]{:S(2)}) collective-permute-start(bf16[64,2048]{1,0:T(8,128)(2,1)} %get-tuple-element.41), channel_id=1, source_target_pairs={{0,2},{1,3},{2,0},{3,1},{4,6},{5,7},{6,4},{7,5},{8,10},{9,11},{10,... | collective-permute-start | bytes 786440 | tf_op jit(solution)/shard_map/ppermute | solution.py:335
  29.7 28.3 %collective-permute-start.1 = (bf16[128,2048]{1,0:T(8,128)(2,1)S(1)}, bf16[128,2048]{1,0:T(8,128)(2,1)S(1)}, u32[]{:S(2)}, u32[]{:S(2)}) collective-permute-start(bf16[128,2048]{1,0:T(8,128)(2,1)S(1)} %copy-done.3), channel_id=1, source_target_pairs={{0,1},{1,2},{2,3},{3,0},{4,5},{5,6},{6,7},{7,4},{8,9},{9,10},{10,1... | collective-permute-start | bytes 1572872 | tf_op jit(solution)/shard_map/ppermute | solution.py:335
  32.3 25.7 %collective-permute-start.3 = (bf16[128,2048]{1,0:T(8,128)(2,1)S(1)}, bf16[128,2048]{1,0:T(8,128)(2,1)S(1)}, u32[]{:S(2)}, u32[]{:S(2)}) collective-permute-start(bf16[128,2048]{1,0:T(8,128)(2,1)S(1)} %copy-done.3), channel_id=1, source_target_pairs={{0,3},{1,0},{2,1},{3,2},{4,7},{5,4},{6,5},{7,6},{8,11},{9,8},{10,9... | collective-permute-start | bytes 1572872 | tf_op jit(solution)/shard_map/ppermute | solution.py:335
  36.8 21.2 %collective-permute-start.4 = (bf16[64,2048]{1,0:T(8,128)(2,1)}, bf16[64,2048]{1,0:T(8,128)(2,1)}, u32[]{:S(2)}, u32[]{:S(2)}) collective-permute-start(bf16[64,2048]{1,0:T(8,128)(2,1)} %get-tuple-element.42), channel_id=1, source_target_pairs={{0,1},{1,2},{2,3},{3,0},{4,5},{5,6},{6,7},{7,4},{8,9},{9,10},{10,1... | collective-permute-start | bytes 786440 | tf_op jit(solution)/shard_map/ppermute | solution.py:335
  38.7 19.4 %copy-start.2 = (bf16[8,256,128]{2,1,0:T(8,128)(2,1)}, bf16[8,256,128]{2,1,0:T(8,128)(2,1)S(1)}, u32[]{:S(2)}) copy-start(bf16[8,256,128]{2,1,0:T(8,128)(2,1)S(1)} %all-to-all-done) | copy-start | bytes 1572868
  40.6 17.4 %collective-permute-start.6 = (bf16[64,2048]{1,0:T(8,128)(2,1)}, bf16[64,2048]{1,0:T(8,128)(2,1)}, u32[]{:S(2)}, u32[]{:S(2)}) collective-permute-start(bf16[64,2048]{1,0:T(8,128)(2,1)} %get-tuple-element.26), channel_id=1, source_target_pairs={{0,3},{1,0},{2,1},{3,2},{4,7},{5,4},{6,5},{7,6},{8,11},{9,8},{10,9... | collective-permute-start | bytes 786440 | tf_op jit(solution)/shard_map/ppermute | solution.py:335
  58.0 21.5 %copy-start.4 = (bf16[128,2048]{1,0:T(8,128)(2,1)}, bf16[128,2048]{1,0:T(8,128)(2,1)S(1)}, u32[]{:S(2)}) copy-start(bf16[128,2048]{1,0:T(8,128)(2,1)S(1)} %collective-permute-done.2.refs_6_) | copy-start | bytes 1572868
  58.0 21.5 %copy-start.5 = (bf16[128,2048]{1,0:T(8,128)(2,1)}, bf16[128,2048]{1,0:T(8,128)(2,1)S(1)}, u32[]{:S(2)}) copy-start(bf16[128,2048]{1,0:T(8,128)(2,1)S(1)} %collective-permute-done.1.refs_5_) | copy-start | bytes 1572868
  58.0 21.4 %copy-start.6 = (bf16[128,2048]{1,0:T(8,128)(2,1)}, bf16[128,2048]{1,0:T(8,128)(2,1)S(1)}, u32[]{:S(2)}) copy-start(bf16[128,2048]{1,0:T(8,128)(2,1)S(1)} %collective-permute-done.3.refs_7_) | copy-start | bytes 1572868
  79.5 27.1 %all-to-all-start.1 = ((bf16[32,136,128]{2,1,0:T(8,128)(2,1)}), bf16[32,136,128]{2,1,0:T(8,128)(2,1)S(1)}, u32[]{:S(2)}, u32[]{:S(2)}) async-start(bf16[32,136,128]{2,1,0:T(8,128)(2,1)} %bitcast.26), calls=%async_computation.1 | async-start | bytes 2228224 | tf_op jit(solution)/shard_map/all_to_all | solution.py:357
  106.6 1.0 copy-start.1
Sparse Core Ops, SparseCore 0:
  9.4 48.3 all-gather.1
